TPU v7x, 512 devices: a 8x2x16 block of a 8x8x16 slice. The times are simulated.
512 devices in a mesh: grp: 2 (over y), sp: 32 (over z, core), tp: 8 (over x).
Axes of the slice: x: 8, y: 2, z: 16, core: 2. Of those that a mesh axis runs over, the one named last changes fastest.
The devices are a block of a 8x8x16 slice.
Arguments:
- tokens: bfloat16 [16384, 4096], P(('grp', 'sp')), parts along dimension 0, may hold values from -6 to 6
- norm_gain: bfloat16 [2, 4096], replicated, may hold values from 0.099609375 to 1.8984375
- w_query: bfloat16 [2, 4096, 2048], P(None, 'sp', 'tp'), may hold values from -0.09375 to 0.09375
- w_key: bfloat16 [2, 4096, 2048], P(None, 'sp', 'tp'), may hold values from -0.09375 to 0.09375
- w_value: bfloat16 [2, 4096, 2048], P(None, 'sp', 'tp'), may hold values from -0.09375 to 0.09375
- w_out: bfloat16 [2, 2048, 4096], P(None, 'tp', 'sp'), may hold values from -0.125 to 0.125
- offset_bias: float32 [2, 16, 15, 31], P(None, 'tp'), may hold values from -4 to 300
Outputs:
- mixed: bfloat16 [16384, 4096], P(('grp', 'sp')), parts along dimension 0
There are 2 independent parts, one for each index of `grp`. A program takes and returns all parts, laid end to end along the dimension named above; an argument that names none is the same for every part. Nothing has to cross between parts.
All inputs are finite; a program needn't handle non-finite values.
Results may differ from a plain program's by a relative error of at most 0.013.
Values may be sent and summed in bfloat16 or wider, within the bound.
A program may use at most 128 MiB of HBM per device.

v0:
```python
import jax
import jax.numpy as jnp
from jax import lax
from jax.sharding import PartitionSpec as P

HD = 128
GRID_W = 64
KR = 8
KC = 16
LAYERS = 2
norm_eps = 1e-06


def turned_gather(arrays, axis, dims):
    turned = [jnp.moveaxis(a, dim, 0) for a, dim in zip(arrays, dims)]
    both = jnp.concatenate([t.reshape(len(t), -1) for t in turned], axis=1)
    result, at, outs = (lax.all_gather(both, axis, axis=0, tiled=True), 0, [])
    for t, dim in zip(turned, dims):
        share = result[:, at : at + t[0].size].reshape(-1, *t.shape[1:])
        outs.append(jnp.moveaxis(share, 0, dim))
        at += t[0].size
    return tuple(outs)


def with_halo(block, sides, width):
    for axis, dim in sides:
        count = lax.axis_size(axis)
        forward = [(i, i + 1) for i in range(count - 1)]
        backward = [(target, source) for source, target in forward]
        low = lax.ppermute(
            lax.slice_in_dim(block, block.shape[dim] - width, None, axis=dim), axis, forward
        )
        high = lax.ppermute(lax.slice_in_dim(block, 0, width, axis=dim), axis, backward)
        block = jnp.concatenate([low, block, high], axis=dim)
    return block


def rms_rows(values, gain):
    wide = values.astype(jnp.float32)
    scaled = wide * lax.rsqrt(jnp.mean(wide * wide, axis=-1, keepdims=True) + norm_eps)
    return (scaled * gain.astype(jnp.float32)).astype(jnp.bfloat16)


def gather_rows(block_rows):
    return lax.all_gather(block_rows, "tp", axis=0, tiled=True)


def on_device(tokens, norm_gain, w_query, w_key, w_value, w_out, offset_bias):
    sp_count = lax.axis_size("sp")
    sp_index = lax.axis_index("sp")
    tp_count = lax.axis_size("tp")
    tp_index = lax.axis_index("tp")
    tok_rows = tokens.shape[0]
    local_rows = tok_rows // GRID_W
    grid_rows = local_rows * sp_count
    heads_here = offset_bias.shape[1]
    head_width = heads_here * HD
    share_rows = tok_rows // tp_count
    reach = KR // 2
    scale = HD ** (-0.5)
    columns = jnp.arange(GRID_W, dtype=jnp.int32)
    col_first = jnp.clip(columns - KC // 2, 0, GRID_W - KC)
    col_inside = (columns[None, :] >= col_first[:, None]) & (
        columns[None, :] < col_first[:, None] + KC
    )
    col_offset = jnp.clip(columns[None, :] - columns[:, None], 1 - KC, KC - 1) + KC - 1
    col_onehot = (
        jnp.arange(2 * KC - 1, dtype=jnp.int32)[:, None, None] == col_offset[None, :, :]
    ).astype(jnp.float32)
    first_row = sp_index * local_rows
    own_rows = first_row + jnp.arange(local_rows, dtype=jnp.int32)
    row_first = jnp.clip(own_rows - reach, 0, grid_rows - KR)
    band_start = row_first - first_row + reach
    row_offset = (
        row_first[:, None] + jnp.arange(KR, dtype=jnp.int32)[None, :] - own_rows[:, None] + KR - 1
    )
    row_onehot = (
        row_offset[:, :, None] == jnp.arange(2 * KR - 1, dtype=jnp.int32)[None, None, :]
    ).astype(jnp.float32)
    every_query, every_key, every_value, every_out = turned_gather(
        (w_query, w_key, w_value, w_out), "sp", (1, 1, 1, 2)
    )
    residual = tokens
    for layer_index in range(LAYERS):
        if layer_index > 0:
            normed = gather_rows(rms_rows(residual, norm_gain[layer_index]))
        else:
            normed = rms_rows(residual, norm_gain[layer_index])
        queries = jnp.dot(normed, every_query[layer_index], preferred_element_type=jnp.float32)
        keys = jnp.dot(normed, every_key[layer_index], preferred_element_type=jnp.float32)
        values = jnp.dot(normed, every_value[layer_index], preferred_element_type=jnp.float32)
        out_weight = every_out[layer_index]
        queries = queries.astype(jnp.bfloat16).reshape(local_rows, GRID_W, heads_here, HD)
        key_values = jnp.concatenate(
            [keys.astype(jnp.bfloat16), values.astype(jnp.bfloat16)], axis=1
        )
        key_values = key_values.reshape(local_rows, GRID_W, 2 * head_width)
        padded = with_halo(key_values, (("sp", 0),), reach)
        bands = jax.vmap(lambda band_begin: lax.dynamic_slice_in_dim(padded, band_begin, KR, 0))(
            band_start
        )
        band_keys = bands[..., :head_width].reshape(local_rows, KR, GRID_W, heads_here, HD)
        band_values = bands[..., head_width:].reshape(local_rows, KR, GRID_W, heads_here, HD)
        col_bias = jnp.einsum(
            "hro,oqk->hrqk", offset_bias[layer_index], col_onehot, precision=lax.Precision.HIGHEST
        )
        full_bias = jnp.einsum(
            "ijr,hrqk->hiqjk", row_onehot, col_bias, precision=lax.Precision.HIGHEST
        )
        scores = jnp.einsum(
            "iqhd,ijkhd->hiqjk", queries, band_keys, preferred_element_type=jnp.float32
        )
        scores = scores * scale + full_bias
        scores = jnp.where(col_inside[None, None, :, None, :], scores, -jnp.inf)
        flattened = scores.reshape(heads_here, local_rows, GRID_W, KR * GRID_W)
        weights = jax.nn.softmax(flattened, axis=-1).astype(jnp.bfloat16)
        weights = weights.reshape(heads_here, local_rows, GRID_W, KR, GRID_W)
        attended = jnp.einsum(
            "hiqjk,ijkhd->iqhd", weights, band_values, preferred_element_type=jnp.float32
        )
        attended = attended.astype(jnp.bfloat16).reshape(tok_rows, head_width)

        def term_rows(row_begin, row_count, attended=attended, out_weight=out_weight):
            return jnp.dot(attended, out_weight, preferred_element_type=jnp.float32)

        branch = lax.psum_scatter(
            term_rows(jnp.int32(0), lax.axis_size("tp") * share_rows).astype(jnp.bfloat16),
            "tp",
            scatter_dimension=0,
            tiled=True,
        ).astype(jnp.float32)
        if layer_index > 0:
            own_part = residual
        else:
            own_part = lax.dynamic_slice_in_dim(tokens, tp_index * share_rows, share_rows, 0)
        residual = (own_part.astype(jnp.float32) + branch).astype(jnp.bfloat16)
    residual = gather_rows(residual)
    return residual


def solution(mesh):
    return jax.shard_map(
        on_device,
        mesh=mesh,
        in_specs=(
            P(("grp", "sp"), None),
            P(),
            P(None, "sp", "tp"),
            P(None, "sp", "tp"),
            P(None, "sp", "tp"),
            P(None, "tp", "sp"),
            P(None, "tp", None, None),
        ),
        out_specs=P(("grp", "sp"), None),
        check_vma=False,
    )
```

profile of v0, /device:TPU:66, one launch (start us, length us, event | category | flops | bytes accessed | tf_op | source)
XLA Modules:
  0.0 439.5 jit_solution(5943801142886471088)
XLA Ops:
  9.7 1.7 pad_maximum_fusion.2
  12.5 2.4 fusion.52
  14.9 2.3 copy.26
  17.8 2.1 fusion
  20.6 156.0 %all-gather.4.cloned.1.call-done = bf16[4096,2048]{0,1:T(8,128)(2,1)} async-done(((bf16[128,2048]{0,1:T(8,128)(2,1)}), bf16[4096,2048]{0,1:T(8,128)(2,1)}) %all-gather.4.cloned.1.call-update) | async-done | bytes 16777232 | tf_op jit(solution)/shard_map/all_gather | solution.py:17
  176.6 10.2 %fusion.60 = (bf16[4096,512]{0,1:T(8,128)(2,1)}, bf16[4096,512]{0,1:T(8,128)(2,1)}, bf16[4096,512]{0,1:T(8,128)(2,1)S(1)}, bf16[4096,512]{0,1:T(8,128)(2,1)S(1)}) fusion(bf16[4096,2048]{0,1:T(8,128)(2,1)} %all-gather.4.cloned.1.call-done), kind=kLoop, calls=%fused_computation.110 | loop fusion | bytes 33554432 | tf_op jit(solution)/shard_map/slice | solution.py:19
  190.1 2.2 collective-permute-start
  192.3 1.3 collective-permute-start.1
  193.7 3.0 fusion.17
  198.6 2.1 gather_fusion
  200.7 1.9 slice_bitcast_fusion.30
  204.2 1.5 copy-done
  205.7 2.0 convolution_convert_fusion.1
  207.9 48.9 %reduce-scatter.3.cloned.1.call-done = bf16[32,4096]{1,0:T(8,128)(2,1)} async-done(((bf16[256,4096]{1,0:T(8,128)(2,1)}), bf16[32,4096]{1,0:T(8,128)(2,1)}) %reduce-scatter.3.cloned.1.call-update) | async-done | bytes 262160 | tf_op jit(solution)/shard_map/reduce_scatter | solution.py:126
  256.9 1.2 fusion.36
  260.0 2.3 fusion.50
  262.3 2.3 copy.33
  264.7 41.1 %all-gather.6.cloned.1.call-done = bf16[256,4096]{1,0:T(8,128)(2,1)} async-done(((bf16[32,4096]{1,0:T(8,128)(2,1)}), bf16[256,4096]{1,0:T(8,128)(2,1)}) %all-gather.6.cloned.1.call-update) | async-done | bytes 2097168 | tf_op jit(solution)/shard_map/all_gather | solution.py:45
  305.8 3.1 fusion.18
  309.2 2.3 fusion.19
  311.8 1.3 collective-permute-start.2
  313.1 1.3 collective-permute-start.3
  314.4 3.0 fusion.20
  318.6 1.2 pad_maximum_fusion.1
  319.8 2.0 gather_fusion.1
  321.8 1.9 slice_bitcast_fusion.28
  325.3 1.5 copy-done.1
  326.8 2.0 convolution_convert_fusion
  329.0 52.1 %reduce-scatter.5.cloned.1.call-done = bf16[32,4096]{1,0:T(8,128)(2,1)} async-done(((bf16[256,4096]{1,0:T(8,128)(2,1)}), bf16[32,4096]{1,0:T(8,128)(2,1)}) %reduce-scatter.5.cloned.1.call-update) | async-done | bytes 262160 | tf_op jit(solution)/shard_map/reduce_scatter | solution.py:126
  381.1 1.7 fusion.39
  382.9 46.9 %all-gather.8.cloned.1.call-done = bf16[256,4096]{1,0:T(8,128)(2,1)} async-done(((bf16[32,4096]{1,0:T(8,128)(2,1)}), bf16[256,4096]{1,0:T(8,128)(2,1)}) %all-gather.8.cloned.1.call-update) | async-done | bytes 2097168 | tf_op jit(solution)/shard_map/all_gather | solution.py:45
  429.8 3.1 copy.111
  (76 shorter events, 17.6 us)
Async XLA Ops:
  6.5 5.0 %copy-start.12 = (f32[2,2,15,31]{3,1,2,0:T(2,128)S(1)}, f32[2,2,15,31]{3,1,2,0:T(2,128)}, u32[]{:S(2)}) copy-start(f32[2,2,15,31]{3,1,2,0:T(2,128)} %param.13) | copy-start | bytes 22324
  6.5 170.0 %all-gather.4.cloned.1.call-start = ((), (), s32[]{:S(2)}) async-start(), calls=%async_computation.2 | async-start | bytes 17301504 | tf_op jit(solution)/shard_map/all_gather | solution.py:17
  11.5 245.4 %reduce-scatter.3.cloned.1.call-start = ((), (), s32[]{:S(2)}) async-start(), calls=%async_computation.3 | async-start | bytes 2359296 | tf_op jit(solution)/shard_map/reduce_scatter | solution.py:126
  12.5 2.4 copy-start.13
  17.2 2.7 copy-start.9
  176.6 10.2 %copy-start.5 = (bf16[256,4096]{1,0:T(8,128)(2,1)S(1)}, bf16[256,4096]{1,0:T(8,128)(2,1)}, u32[]{:S(2)}) copy-start(bf16[256,4096]{1,0:T(8,128)(2,1)} %param.7) | copy-start | bytes 6291460
  186.7 1.9 copy-start.2
  186.7 3.2 copy-start.4
  190.1 6.6 %collective-permute-start = (bf16[4,64,512]{2,1,0:T(8,128)(2,1)S(1)}, bf16[4,64,512]{2,1,0:T(8,128)(2,1)S(1)}, u32[]{:S(2)}, u32[]{:S(2)}) collective-permute-start(bf16[4,64,512]{2,1,0:T(8,128)(2,1)S(1)} %bitcast.167), channel_id=1, source_target_pairs={{0,8},{8,16},{16,24},{24,32},{32,40},{40,48},{48,56},{56,64},{64,7... | collective-permute-start | bytes 786440 | tf_op jit(solution)/shard_map/ppermute | solution.py:30
  192.3 5.1 %collective-permute-start.1 = (bf16[4,64,512]{2,1,0:T(8,128)(2,1)S(1)}, bf16[4,64,512]{2,1,0:T(8,128)(2,1)}, u32[]{:S(2)}, u32[]{:S(2)}) collective-permute-start(bf16[4,64,512]{2,1,0:T(8,128)(2,1)S(1)} %bitcast.168), channel_id=1, source_target_pairs={{8,0},{16,8},{24,16},{32,24},{40,32},{48,40},{56,48},{64,56},{72,6... | collective-permute-start | bytes 786440 | tf_op jit(solution)/shard_map/ppermute | solution.py:33
  196.7 0.7 copy-start.7
  203.6 2.2 copy-start
  207.8 50.3 %copy-start.10 = (f32[1,4096]{1,0:T(1,128)S(1)}, f32[1,4096]{1,0:T(1,128)}, u32[]{:S(2)}) copy-start(f32[1,4096]{1,0:T(1,128)} %get-tuple-element.17) | copy-start | bytes 49156
  207.8 52.2 %copy-start.14 = (s32[4,8]{1,0:T(4,128)S(1)}, s32[4,8]{1,0:T(4,128)}, u32[]{:S(2)}) copy-start(s32[4,8]{1,0:T(4,128)} %copy-done.13) | copy-start | bytes 388
  207.8 97.9 %all-gather.6.cloned.1.call-start = ((), (), s32[]{:S(2)}) async-start(), calls=%async_computation.4 | async-start | bytes 2359296 | tf_op jit(solution)/shard_map/all_gather | solution.py:45
  259.0 122.1 %reduce-scatter.5.cloned.1.call-start = ((), (), s32[]{:S(2)}) async-start(), calls=%async_computation.5 | async-start | bytes 2359296 | tf_op jit(solution)/shard_map/reduce_scatter | solution.py:126
  305.8 3.4 copy-start.3
  311.7 5.6 %copy-start.6 = (bf16[256,512]{1,0:T(8,128)(2,1)}, bf16[256,512]{1,0:T(8,128)(2,1)S(1)}, u32[]{:S(2)}) copy-start(bf16[256,512]{1,0:T(8,128)(2,1)S(1)} %copy.30) | copy-start | bytes 786436
  311.8 8.0 %copy-start.11 = (s32[4]{0:T(128)S(1)}, s32[4]{0:T(128)}, u32[]{:S(2)}) copy-start(s32[4]{0:T(128)} %shift-left_bitcast_fusion) | copy-start | bytes 52
  311.8 5.7 %collective-permute-start.2 = (bf16[4,64,512]{2,1,0:T(8,128)(2,1)S(1)}, bf16[4,64,512]{2,1,0:T(8,128)(2,1)S(1)}, u32[]{:S(2)}, u32[]{:S(2)}) collective-permute-start(bf16[4,64,512]{2,1,0:T(8,128)(2,1)S(1)} %bitcast.170), channel_id=1, source_target_pairs={{0,8},{8,16},{16,24},{24,32},{32,40},{40,48},{48,56},{56,64},{64,7... | collective-permute-start | bytes 786440 | tf_op jit(solution)/shard_map/ppermute | solution.py:30
  313.1 5.5 %collective-permute-start.3 = (bf16[4,64,512]{2,1,0:T(8,128)(2,1)S(1)}, bf16[4,64,512]{2,1,0:T(8,128)(2,1)}, u32[]{:S(2)}, u32[]{:S(2)}) collective-permute-start(bf16[4,64,512]{2,1,0:T(8,128)(2,1)S(1)} %bitcast.171), channel_id=1, source_target_pairs={{8,0},{16,8},{24,16},{32,24},{40,32},{48,40},{56,48},{64,56},{72,6... | collective-permute-start | bytes 786440 | tf_op jit(solution)/shard_map/ppermute | solution.py:33
  317.4 0.7 copy-start.8
  324.6 2.2 copy-start.1
  328.9 100.9 %all-gather.8.cloned.1.call-start = ((), (), s32[]{:S(2)}) async-start(), calls=%async_computation.6 | async-start | bytes 2359296 | tf_op jit(solution)/shard_map/all_gather | solution.py:45
Sparse Core Ops, SparseCore 0:
  11.6 164.9 all-gather.3
  208.0 48.8 reduce-scatter.2
  259.1 46.6 all-gather.5
  329.0 52.0 reduce-scatter.4
  383.1 46.6 all-gather.7
where the time goes:
time: 440 us; the launch traced here: 439 us
  waiting for transfers between devices  346 us (79%)
  local copies, waits for them, and re-layouts  35.7 us (8%)
  matrix products  25.7 us (6%)
  between operations  13.6 us (3%)
  other arithmetic  12.2 us (3%)
  starting transfers between devices  6.58 us (1%)
    all_gather x1, waiting for transfers between devices, turned_gather(): result, at, outs = (lax.all_gather(both, axis, axis=0, tiled=True), 0, [])  156 us
    reduce_scatter x2, waiting for transfers between devices, on_device(): lax.psum_scatter(term_rows(jnp.int32(0), lax.axis_size('tp') * share_rows...  101 us
    all_gather x2, waiting for transfers between devices, gather_rows(): return lax.all_gather(block_rows, 'tp', axis=0, tiled=True)  88 us
    unnamed x36, local copies, waits for them, and re-layouts  16.1 us
    slice x1, local copies, waits for them, and re-layouts, turned_gather(): share = result[:, at:at + t[0].size].reshape(-1, *t.shape[1:])  10.2 us
  transfers between devices with their start and end apart: 9, of which 6 were waited for; matrix products, arithmetic and copies ran while one was open for 5% of the time, Pallas kernels for 0%

commit v1 on v0

--- a/solution.py
+++ b/solution.py
@@ -9,6 +9,11 @@
 KC = 16
 LAYERS = 2
 norm_eps = 1e-06
+
+
+def tiled_gather(array, axis, dim):
+    copies = jnp.concatenate([array] * lax.axis_size(axis), axis=dim)
+    return lax.all_to_all(copies, axis, dim, dim, tiled=True)
 
 
 def turned_gather(arrays, axis, dims):
@@ -42,7 +47,7 @@
 
 
 def gather_rows(block_rows):
-    return lax.all_gather(block_rows, "tp", axis=0, tiled=True)
+    return tiled_gather(block_rows, "tp", 0)
 
 
 def on_device(tokens, norm_gain, w_query, w_key, w_value, w_out, offset_bias):

time: 440 us -> 451 us (1.025)
  blocking collectives: 0 us -> 51.3 us
  waiting for transfers between devices: 346 us -> 297 us
  starting transfers between devices: 6.58 us -> 11.8 us
    all_gather x2 -> x0, waiting for transfers between devices: 88 us -> none  [gather_rows(): return lax.all_gather(block_rows, 'tp', axis=0, tiled=True)]
    all_to_all x0 -> x1, blocking collectives: none -> 51.3 us  [tiled_gather(): return lax.all_to_all(copies, axis, dim, dim, tiled=True)]
    all_to_all x0 -> x1, waiting for transfers between devices: none -> 40.8 us  [tiled_gather(): return lax.all_to_all(copies, axis, dim, dim, tiled=True)]
    unnamed x0 -> x8, other arithmetic: none -> 6.84 us
    all_to_all x0 -> x1, starting transfers between devices: none -> 5.57 us  [tiled_gather(): return lax.all_to_all(copies, axis, dim, dim, tiled=True)]
    unnamed x36 -> x40, local copies, waits for them, and re-layouts: 16.1 us -> 15 us
  transfers between devices with their start and end apart: 9 -> 8, of which waited for: 6 -> 5; matrix products, arithmetic and copies ran while one was open for 5% -> 5% of each run, Pallas kernels for 0% -> 0%
where the time goes in v1:
time: 451 us
  waiting for transfers between devices  297 us (66%)
  blocking collectives  51.3 us (11%)
  local copies, waits for them, and re-layouts  35.2 us (8%)
  matrix products  25.7 us (6%)
  other arithmetic  16.5 us (4%)
  between operations  13.6 us (3%)
  starting transfers between devices  11.8 us (3%)
    all_gather x1, waiting for transfers between devices, turned_gather(): result, at, outs = (lax.all_gather(both, axis, axis=0, tiled=True), 0, [])  155 us
    reduce_scatter x2, waiting for transfers between devices, on_device(): lax.psum_scatter(term_rows(jnp.int32(0), lax.axis_size('tp') * share_rows...  99.9 us
    all_to_all x1, blocking collectives, tiled_gather(): return lax.all_to_all(copies, axis, dim, dim, tiled=True)  51.3 us
    all_to_all x1, waiting for transfers between devices, tiled_gather(): return lax.all_to_all(copies, axis, dim, dim, tiled=True)  40.8 us
    unnamed x40, local copies, waits for them, and re-layouts  15 us
    slice x1, local copies, waits for them, and re-layouts, turned_gather(): share = result[:, at:at + t[0].size].reshape(-1, *t.shape[1:])  10.2 us
  transfers between devices with their start and end apart: 8, of which 5 were waited for; matrix products, arithmetic and copies ran while one was open for 5% of the time, Pallas kernels for 0%

profile of v1, /device:TPU:66, one launch (start us, length us, event | category | flops | bytes accessed | tf_op | source)
XLA Modules:
  0.0 450.7 jit_solution(13433619927641621776)
XLA Ops:
  9.7 1.7 pad_maximum_fusion.2
  13.7 2.3 fusion.52
  16.0 2.3 copy.26
  18.9 2.1 fusion
  21.1 155.5 %all-gather.2.cloned.1.call-done = bf16[4096,2048]{0,1:T(8,128)(2,1)} async-done(((bf16[128,2048]{0,1:T(8,128)(2,1)}), bf16[4096,2048]{0,1:T(8,128)(2,1)}) %all-gather.2.cloned.1.call-update) | async-done | bytes 16777232 | tf_op jit(solution)/shard_map/all_gather | solution.py:22
  176.6 10.2 %fusion.61 = (bf16[4096,512]{0,1:T(8,128)(2,1)}, bf16[4096,512]{0,1:T(8,128)(2,1)}, bf16[4096,512]{0,1:T(8,128)(2,1)S(1)}, bf16[4096,512]{0,1:T(8,128)(2,1)S(1)}) fusion(bf16[4096,2048]{0,1:T(8,128)(2,1)} %all-gather.2.cloned.1.call-done), kind=kLoop, calls=%fused_computation.126 | loop fusion | bytes 33554432 | tf_op jit(solution)/shard_map/slice | solution.py:24
  190.1 2.2 collective-permute-start
  192.3 1.3 collective-permute-start.1
  193.6 3.0 fusion.17
  197.4 1.1 pad_maximum_fusion
  198.5 2.1 gather_fusion
  200.7 1.9 slice_bitcast_fusion.30
  204.2 1.5 copy-done
  205.7 2.0 convolution_convert_fusion.1
  207.8 49.0 %reduce-scatter.3.cloned.1.call-done = bf16[32,4096]{1,0:T(8,128)(2,1)} async-done(((bf16[256,4096]{1,0:T(8,128)(2,1)}), bf16[32,4096]{1,0:T(8,128)(2,1)}) %reduce-scatter.3.cloned.1.call-update) | async-done | bytes 262160 | tf_op jit(solution)/shard_map/reduce_scatter | solution.py:131
  256.9 1.2 fusion.36
  264.8 5.6 %all-to-all-start = ((bf16[8,32,4096]{2,1,0:T(8,128)(2,1)}), bf16[8,32,4096]{2,1,0:T(8,128)(2,1)}, u32[]{:S(2)}, u32[]{:S(2)}) async-start(bf16[8,32,4096]{2,1,0:T(8,128)(2,1)} %bitcast.37), calls=%async_computation.1 | async-start | bytes 4194304 | tf_op jit(solution)/shard_map/all_to_all | solution.py:16
  271.1 2.4 fusion.50
  273.4 2.3 copy.33
  275.8 40.8 %all-to-all-done = bf16[8,32,4096]{2,1,0:T(8,128)(2,1)} async-done(((bf16[8,32,4096]{2,1,0:T(8,128)(2,1)}), bf16[8,32,4096]{2,1,0:T(8,128)(2,1)}, u32[]{:S(2)}, u32[]{:S(2)}) %all-to-all-start) | async-done | bytes 2097184 | tf_op jit(solution)/shard_map/all_to_all | solution.py:16
  316.6 3.1 fusion.18
  320.0 2.3 fusion.19
  322.5 1.3 collective-permute-start.2
  323.9 1.3 collective-permute-start.3
  325.2 3.0 fusion.20
  330.4 2.0 gather_fusion.1
  332.4 1.9 slice_bitcast_fusion.28
  335.9 1.5 copy-done.1
  337.4 2.0 convolution_convert_fusion
  339.5 50.8 %reduce-scatter.5.cloned.1.call-done = bf16[32,4096]{1,0:T(8,128)(2,1)} async-done(((bf16[256,4096]{1,0:T(8,128)(2,1)}), bf16[32,4096]{1,0:T(8,128)(2,1)}) %reduce-scatter.5.cloned.1.call-update) | async-done | bytes 262160 | tf_op jit(solution)/shard_map/reduce_scatter | solution.py:131
  391.6 51.3 %all_to_all.24 = bf16[8,32,4096]{2,1,0:T(8,128)(2,1)S(1)} all-to-all(bf16[8,32,4096]{2,1,0:T(8,128)(2,1)S(1)} %bitcast.172), channel_id=1, replica_groups=mesh['grp'=2,'sp'=32,'tp'=8] {'tp'}, dimensions={0} | all-to-all | bytes 4194304 | tf_op jit(solution)/shard_map/all_to_all | solution.py:16
  442.9 1.3 copy.125
  (85 shorter events, 24.5 us)
Async XLA Ops:
  6.5 5.0 %copy-start.11 = (f32[2,2,15,31]{3,1,2,0:T(2,128)S(1)}, f32[2,2,15,31]{3,1,2,0:T(2,128)}, u32[]{:S(2)}) copy-start(f32[2,2,15,31]{3,1,2,0:T(2,128)} %param.13) | copy-start | bytes 22324
  6.5 170.0 %all-gather.2.cloned.1.call-start = ((), (), s32[]{:S(2)}) async-start(), calls=%async_computation.4 | async-start | bytes 17301504 | tf_op jit(solution)/shard_map/all_gather | solution.py:22
  11.5 245.4 %reduce-scatter.3.cloned.1.call-start = ((), (), s32[]{:S(2)}) async-start(), calls=%async_computation.5 | async-start | bytes 2359296 | tf_op jit(solution)/shard_map/reduce_scatter | solution.py:131
  13.1 0.6 copy-start.12
  18.4 2.7 copy-start.9
  176.6 10.2 %copy-start.5 = (bf16[256,4096]{1,0:T(8,128)(2,1)S(1)}, bf16[256,4096]{1,0:T(8,128)(2,1)}, u32[]{:S(2)}) copy-start(bf16[256,4096]{1,0:T(8,128)(2,1)} %param.7) | copy-start | bytes 6291460
  186.7 2.0 copy-start.2
  186.7 3.2 copy-start.4
  190.1 6.6 %collective-permute-start = (bf16[4,64,512]{2,1,0:T(8,128)(2,1)S(1)}, bf16[4,64,512]{2,1,0:T(8,128)(2,1)S(1)}, u32[]{:S(2)}, u32[]{:S(2)}) collective-permute-start(bf16[4,64,512]{2,1,0:T(8,128)(2,1)S(1)} %bitcast.181), channel_id=1, source_target_pairs={{0,8},{8,16},{16,24},{24,32},{32,40},{40,48},{48,56},{56,64},{64,7... | collective-permute-start | bytes 786440 | tf_op jit(solution)/shard_map/ppermute | solution.py:35
  192.3 5.1 %collective-permute-start.1 = (bf16[4,64,512]{2,1,0:T(8,128)(2,1)S(1)}, bf16[4,64,512]{2,1,0:T(8,128)(2,1)}, u32[]{:S(2)}, u32[]{:S(2)}) collective-permute-start(bf16[4,64,512]{2,1,0:T(8,128)(2,1)S(1)} %bitcast.182), channel_id=1, source_target_pairs={{8,0},{16,8},{24,16},{32,24},{40,32},{48,40},{56,48},{64,56},{72,6... | collective-permute-start | bytes 786440 | tf_op jit(solution)/shard_map/ppermute | solution.py:38
  196.7 0.7 copy-start.6
  203.5 2.2 copy-start
  264.8 5.6 %copy-start.8 = (f32[2,15,31,1]{2,0,1,3:T(2,128)S(1)}, f32[2,15,31,1]{2,0,1,3:T(2,128)}, u32[]{:S(2)}) copy-start(f32[2,15,31,1]{2,0,1,3:T(2,128)} %get-tuple-element.17) | copy-start | bytes 11164
  264.8 6.3 %copy-start.13 = (s32[4,8]{1,0:T(4,128)S(1)}, s32[4,8]{1,0:T(4,128)}, u32[]{:S(2)}) copy-start(s32[4,8]{1,0:T(4,128)} %copy-done.12) | copy-start | bytes 388
  264.8 51.8 %all-to-all-start = ((bf16[8,32,4096]{2,1,0:T(8,128)(2,1)}), bf16[8,32,4096]{2,1,0:T(8,128)(2,1)}, u32[]{:S(2)}, u32[]{:S(2)}) async-start(bf16[8,32,4096]{2,1,0:T(8,128)(2,1)} %bitcast.37), calls=%async_computation.1 | async-start | bytes 4194304 | tf_op jit(solution)/shard_map/all_to_all | solution.py:16
  270.3 120.0 %reduce-scatter.5.cloned.1.call-start = ((), (), s32[]{:S(2)}) async-start(), calls=%async_computation.6 | async-start | bytes 2359296 | tf_op jit(solution)/shard_map/reduce_scatter | solution.py:131
  316.6 3.4 copy-start.3
  322.5 7.8 %copy-start.10 = (s32[4]{0:T(128)S(1)}, s32[4]{0:T(128)}, u32[]{:S(2)}) copy-start(s32[4]{0:T(128)} %shift-left_bitcast_fusion) | copy-start | bytes 52
  322.5 5.7 %collective-permute-start.2 = (bf16[4,64,512]{2,1,0:T(8,128)(2,1)S(1)}, bf16[4,64,512]{2,1,0:T(8,128)(2,1)S(1)}, u32[]{:S(2)}, u32[]{:S(2)}) collective-permute-start(bf16[4,64,512]{2,1,0:T(8,128)(2,1)S(1)} %bitcast.184), channel_id=1, source_target_pairs={{0,8},{8,16},{16,24},{24,32},{32,40},{40,48},{48,56},{56,64},{64,7... | collective-permute-start | bytes 786440 | tf_op jit(solution)/shard_map/ppermute | solution.py:35
  323.9 5.4 %collective-permute-start.3 = (bf16[4,64,512]{2,1,0:T(8,128)(2,1)S(1)}, bf16[4,64,512]{2,1,0:T(8,128)(2,1)}, u32[]{:S(2)}, u32[]{:S(2)}) collective-permute-start(bf16[4,64,512]{2,1,0:T(8,128)(2,1)S(1)} %bitcast.185), channel_id=1, source_target_pairs={{8,0},{16,8},{24,16},{32,24},{40,32},{48,40},{56,48},{64,56},{72,6... | collective-permute-start | bytes 786440 | tf_op jit(solution)/shard_map/ppermute | solution.py:38
  328.2 0.7 copy-start.7
  335.2 2.2 copy-start.1
Sparse Core Ops, SparseCore 0:
  11.6 164.9 all-gather.1
  207.9 48.8 reduce-scatter.2
  339.7 50.6 reduce-scatter.4
